TPU v7x, 128 devices: a whole 4x4x4 slice. The times are simulated.
128 devices in a mesh: ra: 16 (over z, y), cb: 4 (over x), dp: 2 (over core).
Axes of the slice: x: 4, y: 4, z: 4, core: 2. Of those that a mesh axis runs over, the one named last changes fastest.
Arguments:
- tokens: bfloat16 [3072, 4096], P('dp', 'ra'), may hold values from -20 to 20
- pre_gain: float32 [4096], P('ra'), may hold values from 0.1 to 1.9
- up_weight: bfloat16 [4096, 16384], P('ra', 'cb'), may hold values from -0.09375 to 0.09375
- up_bias: float32 [16384], P('cb'), may hold values from -4 to 4
- down_weight: bfloat16 [16384, 4096], P('cb', 'ra'), may hold values from -0.046875 to 0.046875
- post_gain: float32 [4096], P('ra'), may hold values from 0.1 to 1.9
Outputs:
- stream_out: bfloat16 [3072, 4096], P('dp', 'ra')
All inputs are finite; a program needn't handle non-finite values.
Results may differ from a plain program's by a relative error of at most 0.0051.
Values may be sent and summed in bfloat16 or wider, within the bound.
A program may use at most 128 MiB of HBM per device.

v0:
```python
import jax
import jax.numpy as jnp
from jax import lax
from jax.sharding import PartitionSpec as P

D = 4096
epsilon = 1e-06
residual_weight = 0.5


def in_blocks(array, dim, size):
    before, after = (array.shape[:dim], array.shape[dim + 1 :])
    return jnp.moveaxis(array.reshape(*before, size, -1, *after), dim, 0)


def sent_and_summed(array, axis, dim):
    size = lax.axis_size(axis)
    pieces = lax.all_to_all(in_blocks(array, dim, size), axis, 0, 0, tiled=True)
    return jnp.sum(pieces, axis=0)


def from_everyone(array, axis):
    copies = jnp.broadcast_to(array, (lax.axis_size(axis), *array.shape))
    return lax.all_to_all(copies, axis, split_axis=0, concat_axis=0, tiled=True)


def of_everyone(array, axis):
    return from_everyone(array, axis).sum(axis=0)


def activate(summed, inverse, offset):
    return jnp.square(jax.nn.relu(summed * inverse[:, None] + offset)).astype(jnp.bfloat16)


def body(tokens, pre_gain, up_weight, up_bias, down_weight, post_gain):
    stream = tokens.astype(jnp.float32)
    energy = jnp.sum(stream * stream, axis=1)
    scaled = (stream * pre_gain).astype(jnp.bfloat16)
    partial_value = jnp.dot(scaled, up_weight, preferred_element_type=jnp.float32)
    total = sent_and_summed(energy, "ra", 0)
    share = lax.psum_scatter(partial_value, "ra", scatter_dimension=0, tiled=True)
    hidden = activate(share, lax.rsqrt(total / D + epsilon), up_bias)
    branch = jnp.dot(
        lax.all_gather(hidden, "ra", axis=0, tiled=True),
        down_weight,
        preferred_element_type=jnp.float32,
    )
    branch = lax.psum(branch, "cb")
    branch_energy = of_everyone(jnp.sum(branch * branch, axis=1), "ra")
    normed = branch * lax.rsqrt(branch_energy / D + epsilon)[:, None] * post_gain
    return (residual_weight * stream + normed).astype(jnp.bfloat16)


def solution(mesh):
    in_specs = (P("dp", "ra"), P("ra"), P("ra", "cb"), P("cb"), P("cb", "ra"), P("ra"))
    out_specs = P("dp", "ra")
    return jax.shard_map(body, mesh=mesh, in_specs=in_specs, out_specs=out_specs, check_vma=False)
```

profile of v0, /device:TPU:0, one launch (start us, length us, event | category | flops | bytes accessed | tf_op | source)
XLA Modules:
  0.0 353.1 jit_solution(17508895634542770596)
XLA Ops:
  6.5 0.0 copy-start
  6.5 0.0 reduce-scatter.2.cloned.1.call-start
  6.5 1.6 copy-done
  8.1 11.2 %fusion.4 = f32[1536,4096]{1,0:T(8,128)} fusion(bf16[256,4096]{1,0:T(8,128)(2,1)S(1)} %copy-done, bf16[1536,256]{1,0:T(8,128)(2,1)} %param.6, f32[256]{0:T(256)} %param.7), kind=kOutput, calls=%fused_computation.9 | convolution fusion | flops 3222405120 | bytes 28050432 | tf_op jit(solution)/shard_map/dot_general | solution.py:39
  19.4 0.0 copy-start.1
  19.4 0.0 copy-start.2
  19.4 0.0 reduce-scatter.2.cloned.1.call-update
  19.4 0.0 all-gather.2.cloned.1.call-start
  19.4 1.1 copy-done.1
  20.5 0.3 fusion.3
  20.8 0.1 all_to_all.10
  20.9 15.5 %all_to_all.15 = f32[16,1,96]{2,1,0:T(1,128)S(1)} all-to-all(f32[16,1,96]{2,1,0:T(1,128)S(1)} %all_to_all.10), channel_id=1, replica_groups=mesh['ra'=16,'cb'=4,'dp'=2] {'ra'}, dimensions={0} | all-to-all | bytes 12288 | tf_op jit(solution)/shard_map/all_to_all | solution.py:18
  36.4 138.9 %reduce-scatter.2.cloned.1.call-done = f32[96,4096]{1,0:T(8,128)} async-done(((f32[1536,4096]{1,0:T(8,128)}), f32[96,4096]{1,0:T(8,128)}) %reduce-scatter.2.cloned.1.call-update) | async-done | bytes 1572880 | tf_op jit(solution)/shard_map/reduce_scatter | solution.py:41
  175.3 0.0 copy-done.2
  175.3 2.6 multiply_convert_fusion
  177.9 0.0 all-gather.2.cloned.1.call-update
  178.0 0.0 all-reduce.2.cloned.1.call-start
  178.0 89.6 %all-gather.2.cloned.1.call-done = bf16[1536,4096]{1,0:T(8,128)(2,1)} async-done(((bf16[96,4096]{1,0:T(8,128)(2,1)}), bf16[1536,4096]{1,0:T(8,128)(2,1)}) %all-gather.2.cloned.1.call-update) | async-done | bytes 12582928 | tf_op jit(solution)/shard_map/all_gather | solution.py:44
  267.6 9.8 %fusion.7 = f32[1536,256]{1,0:T(8,128)} fusion(bf16[1536,4096]{1,0:T(8,128)(2,1)} %all-gather.2.cloned.1.call-done, bf16[4096,256]{1,0:T(8,128)(2,1)} %param.10), kind=kOutput, calls=%fused_computation.13 | convolution fusion | flops 3221225472 | bytes 16252928 | tf_op jit(solution)/shard_map/dot_general | solution.py:43
  277.4 0.0 copy-start.3
  277.4 0.0 all-reduce.2.cloned.1.call-update
  277.4 50.1 %all-reduce.2.cloned.1.call-done = f32[1536,256]{1,0:T(8,128)} async-done(((f32[1536,256]{1,0:T(8,128)}), f32[1536,256]{1,0:T(8,128)}) %all-reduce.2.cloned.1.call-update) | async-done | bytes 1572880 | tf_op jit(solution)/shard_map/psum | solution.py:48
  327.5 1.7 multiply_reduce_fusion
  329.2 0.1 broadcast_in_dim.2
  329.3 14.6 %all_to_all.16 = f32[16,1,1536]{2,1,0:T(1,128)S(1)} all-to-all(f32[16,1,1536]{2,1,0:T(1,128)S(1)} %broadcast_in_dim.2), channel_id=1, replica_groups=mesh['ra'=16,'cb'=4,'dp'=2] {'ra'}, dimensions={0} | all-to-all | bytes 196608 | tf_op jit(solution)/shard_map/all_to_all | solution.py:24
  343.9 0.1 reduce_sum.39
  343.9 0.0 copy-done.3
  343.9 2.6 fusion.1
  (3 shorter events, 0.0 us)
Async XLA Ops:
  6.5 1.6 copy-start
  6.5 168.8 %reduce-scatter.2.cloned.1.call-start = ((), (), s32[]{:S(2)}) async-start(), calls=%async_computation.3 | async-start | bytes 26738688 | tf_op jit(solution)/shard_map/reduce_scatter | solution.py:41
  19.4 1.1 copy-start.1
  19.4 156.0 %copy-start.2 = (f32[4096]{0:T(1024)S(1)}, f32[4096]{0:T(1024)}, u32[]{:S(2)}) copy-start(f32[4096]{0:T(1024)} %param.9) | copy-start | bytes 49156
  19.4 248.2 %all-gather.2.cloned.1.call-start = ((), (), s32[]{:S(2)}) async-start(), calls=%async_computation.4 | async-start | bytes 13369344 | tf_op jit(solution)/shard_map/all_gather | solution.py:44
  178.0 149.6 %all-reduce.2.cloned.1.call-start = ((), (), s32[]{:S(2)}) async-start(), calls=%async_computation.5 | async-start | bytes 3145728 | tf_op jit(solution)/shard_map/psum | solution.py:48
  277.4 66.5 %copy-start.3 = (f32[256]{0:T(256)S(1)}, f32[256]{0:T(256)}, u32[]{:S(2)}) copy-start(f32[256]{0:T(256)} %param.11) | copy-start | bytes 3076
Sparse Core Ops, SparseCore 0:
  19.5 155.7 reduce-scatter.1
  178.1 89.4 all-gather.1
  277.6 49.8 all-reduce.1
where the time goes:
time: 353 us
  waiting for transfers between devices  279 us (79%)
  blocking collectives  30.1 us (9%)
  matrix products  21.1 us (6%)
  between operations  13.2 us (4%)
  other arithmetic  7.27 us (2%)
    reduce_scatter x1, waiting for transfers between devices, body(): lax.psum_scatter(partial_value, 'ra', scatter_dimension=0, tiled=True)  139 us
    all_gather x1, waiting for transfers between devices, body(): lax.all_gather(hidden, 'ra', axis=0, tiled=True)  89.6 us
    psum x1, waiting for transfers between devices, body(): branch = lax.psum(branch, 'cb')  50.1 us
    all_to_all x1, blocking collectives, sent_and_summed(): pieces = lax.all_to_all(in_blocks(array, dim, size), axis, 0, 0, tiled=True)  15.5 us
    all_to_all x1, blocking collectives, from_everyone(): return lax.all_to_all(copies, axis, split_axis=0, concat_axis=0, tiled=True)  14.6 us
    dot_general x1, matrix products, body(): jnp.dot(scaled, up_weight, preferred_element_type=jnp.float32)  11.2 us
    dot_general x1, matrix products, body(): jnp.dot(lax.all_gather(hidden, 'ra', axis=0, tiled=True), down_weight, pr...  9.83 us
  transfers between devices with their start and end apart: 3, of which 3 were waited for; matrix products, arithmetic and copies ran while one was open for 0% of the time, Pallas kernels for 0%

commit v1 on v0

--- a/solution.py
+++ b/solution.py
@@ -6,6 +6,11 @@
 D = 4096
 epsilon = 1e-06
 residual_weight = 0.5
+
+
+def tiled_gather(array, axis, dim):
+    copies = jnp.concatenate([array] * lax.axis_size(axis), axis=dim)
+    return lax.all_to_all(copies, axis, dim, dim, tiled=True)
 
 
 def in_blocks(array, dim, size):
@@ -40,11 +45,7 @@
     total = sent_and_summed(energy, "ra", 0)
     share = lax.psum_scatter(partial_value, "ra", scatter_dimension=0, tiled=True)
     hidden = activate(share, lax.rsqrt(total / D + epsilon), up_bias)
-    branch = jnp.dot(
-        lax.all_gather(hidden, "ra", axis=0, tiled=True),
-        down_weight,
-        preferred_element_type=jnp.float32,
-    )
+    branch = jnp.dot(tiled_gather(hidden, "ra", 0), down_weight, preferred_element_type=jnp.float32)
     branch = lax.psum(branch, "cb")
     branch_energy = of_everyone(jnp.sum(branch * branch, axis=1), "ra")
     normed = branch * lax.rsqrt(branch_energy / D + epsilon)[:, None] * post_gain

time: 353 us -> 403 us (1.14)
  blocking collectives: 30.1 us -> 176 us
  waiting for transfers between devices: 279 us -> 187 us
  matrix products: 21.1 us -> 16 us
    all_to_all x0 -> x1, blocking collectives: none -> 146 us  [tiled_gather(): return lax.all_to_all(copies, axis, dim, dim, tiled=True)]
    all_gather x1 -> x0, waiting for transfers between devices: 89.6 us -> none  [body(): lax.all_gather(hidden, 'ra', axis=0, tiled=True)]
    dot_general x1, matrix products: 9.83 us -> 4.74 us  [body(): jnp.dot(tiled_gather(hidden, 'ra', 0), down_weight, preferred_element_typ...]
  transfers between devices with their start and end apart: 3 -> 2, of which waited for: 3 -> 2; matrix products, arithmetic and copies ran while one was open for 0% -> 0% of each run, Pallas kernels for 0% -> 0%
where the time goes in v1:
time: 403 us
  waiting for transfers between devices  187 us (46%)
  blocking collectives  176 us (44%)
  matrix products  16 us (4%)
  between operations  13.6 us (3%)
  other arithmetic  6.45 us (2%)
    all_to_all x1, blocking collectives, tiled_gather(): return lax.all_to_all(copies, axis, dim, dim, tiled=True)  146 us
    reduce_scatter x1, waiting for transfers between devices, body(): lax.psum_scatter(partial_value, 'ra', scatter_dimension=0, tiled=True)  139 us
    psum x1, waiting for transfers between devices, body(): branch = lax.psum(branch, 'cb')  48 us
    all_to_all x1, blocking collectives, sent_and_summed(): pieces = lax.all_to_all(in_blocks(array, dim, size), axis, 0, 0, tiled=True)  15.5 us
    all_to_all x1, blocking collectives, from_everyone(): return lax.all_to_all(copies, axis, split_axis=0, concat_axis=0, tiled=True)  14.6 us
    dot_general x1, matrix products, body(): jnp.dot(scaled, up_weight, preferred_element_type=jnp.float32)  11.2 us
  transfers between devices with their start and end apart: 2, of which 2 were waited for; matrix products, arithmetic and copies ran while one was open for 0% of the time, Pallas kernels for 0%

profile of v1, /device:TPU:0, one launch (start us, length us, event | category | flops | bytes accessed | tf_op | source)
XLA Modules:
  0.0 402.6 jit_solution(6418913460021807546)
XLA Ops:
  6.5 1.6 copy-done
  8.1 11.2 %fusion.4 = f32[1536,4096]{1,0:T(8,128)} fusion(bf16[256,4096]{1,0:T(8,128)(2,1)S(1)} %copy-done, bf16[1536,256]{1,0:T(8,128)(2,1)} %param.6, f32[256]{0:T(256)} %param.7), kind=kOutput, calls=%fused_computation.9 | convolution fusion | flops 3222405120 | bytes 28050432 | tf_op jit(solution)/shard_map/dot_general | solution.py:44
  19.4 0.0 all-reduce.2.cloned.1.call-start
  19.4 1.1 copy-done.1
  20.5 0.3 fusion.3
  20.8 0.1 all_to_all.18
  20.9 15.5 %all_to_all.27 = f32[16,1,96]{2,1,0:T(1,128)S(1)} all-to-all(f32[16,1,96]{2,1,0:T(1,128)S(1)} %all_to_all.18), channel_id=1, replica_groups=mesh['ra'=16,'cb'=4,'dp'=2] {'ra'}, dimensions={0} | all-to-all | bytes 12288 | tf_op jit(solution)/shard_map/all_to_all | solution.py:23
  36.4 138.9 %reduce-scatter.2.cloned.1.call-done = f32[96,4096]{1,0:T(8,128)} async-done(((f32[1536,4096]{1,0:T(8,128)}), f32[96,4096]{1,0:T(8,128)}) %reduce-scatter.2.cloned.1.call-update) | async-done | bytes 1572880 | tf_op jit(solution)/shard_map/reduce_scatter | solution.py:46
  175.3 1.8 constant_dynamic-update-slice_fusion.15
  177.1 0.1 constant_dynamic-update-slice_fusion.14
  177.2 0.1 constant_dynamic-update-slice_fusion.13
  177.2 0.1 constant_dynamic-update-slice_fusion.12
  177.3 0.1 constant_dynamic-update-slice_fusion.11
  177.4 0.1 constant_dynamic-update-slice_fusion.10
  177.4 0.1 constant_dynamic-update-slice_fusion.9
  177.5 0.1 constant_dynamic-update-slice_fusion.8
  177.5 0.1 constant_dynamic-update-slice_fusion.7
  177.6 0.1 constant_dynamic-update-slice_fusion.6
  177.7 0.1 constant_dynamic-update-slice_fusion.5
  177.7 0.1 constant_dynamic-update-slice_fusion.4
  177.8 0.1 constant_dynamic-update-slice_fusion.3
  177.8 0.1 constant_dynamic-update-slice_fusion.2
  177.9 0.1 constant_dynamic-update-slice_fusion.1
  178.0 0.1 constant_dynamic-update-slice_fusion
  178.0 145.9 %all_to_all.28 = bf16[16,96,4096]{2,1,0:T(8,128)(2,1)S(1)} all-to-all(bf16[16,96,4096]{2,1,0:T(8,128)(2,1)S(1)} %bitcast.6), channel_id=1, replica_groups=mesh['ra'=16,'cb'=4,'dp'=2] {'ra'}, dimensions={0} | all-to-all | bytes 25165824 | tf_op jit(solution)/shard_map/all_to_all | solution.py:13
  323.9 4.7 %fusion.7 = f32[1536,256]{1,0:T(8,128)} fusion(bf16[1536,4096]{1,0:T(8,128)(2,1)S(1)} %bitcast.7, bf16[4096,256]{1,0:T(8,128)(2,1)S(1)} %copy-done.4), kind=kOutput, calls=%fused_computation.29 | convolution fusion | flops 3221225472 | bytes 16252928 | tf_op jit(solution)/shard_map/dot_general | solution.py:48
  328.7 48.0 %all-reduce.2.cloned.1.call-done = f32[1536,256]{1,0:T(8,128)} async-done(((f32[1536,256]{1,0:T(8,128)}), f32[1536,256]{1,0:T(8,128)}) %all-reduce.2.cloned.1.call-update) | async-done | bytes 1572880 | tf_op jit(solution)/shard_map/psum | solution.py:49
  376.7 1.7 multiply_reduce_fusion
  378.4 0.1 broadcast_in_dim.2
  378.4 14.6 %all_to_all.29 = f32[16,1,1536]{2,1,0:T(1,128)S(1)} all-to-all(f32[16,1,1536]{2,1,0:T(1,128)S(1)} %broadcast_in_dim.2), channel_id=1, replica_groups=mesh['ra'=16,'cb'=4,'dp'=2] {'ra'}, dimensions={0} | all-to-all | bytes 196608 | tf_op jit(solution)/shard_map/all_to_all | solution.py:29
  393.0 0.1 reduce_sum.39
  393.1 2.6 fusion.1
  (14 shorter events, 0.1 us)
Async XLA Ops:
  6.5 1.6 copy-start
  6.5 168.8 %reduce-scatter.2.cloned.1.call-start = ((), (), s32[]{:S(2)}) async-start(), calls=%async_computation.4 | async-start | bytes 26738688 | tf_op jit(solution)/shard_map/reduce_scatter | solution.py:46
  19.4 1.1 copy-start.1
  19.4 156.0 %copy-start.2 = (f32[4096]{0:T(1024)S(1)}, f32[4096]{0:T(1024)}, u32[]{:S(2)}) copy-start(f32[4096]{0:T(1024)} %param.9) | copy-start | bytes 49156
  19.4 357.3 %all-reduce.2.cloned.1.call-start = ((), (), s32[]{:S(2)}) async-start(), calls=%async_computation.5 | async-start | bytes 3145728 | tf_op jit(solution)/shard_map/psum | solution.py:49
  178.0 145.9 %copy-start.4 = (bf16[4096,256]{1,0:T(8,128)(2,1)S(1)}, bf16[4096,256]{1,0:T(8,128)(2,1)}, u32[]{:S(2)}) copy-start(bf16[4096,256]{1,0:T(8,128)(2,1)} %param.10) | copy-start | bytes 6291460
  323.9 69.2 %copy-start.3 = (f32[256]{0:T(256)S(1)}, f32[256]{0:T(256)}, u32[]{:S(2)}) copy-start(f32[256]{0:T(256)} %param.11) | copy-start | bytes 3076
Sparse Core Ops, SparseCore 0:
  19.5 155.7 reduce-scatter.1
  328.8 47.7 all-reduce.1
